TPU v7x, 32 devices: a whole 2x2x4 slice. The times are simulated.
32 devices in a mesh: sp: 16 (over z, y, x), tp: 2 (over core).
Axes of the slice: x: 2, y: 2, z: 4, core: 2. Of those that a mesh axis runs over, the one named last changes fastest.
Arguments:
- hidden_in: bfloat16 [4096, 2048], P('sp', 'tp'), may hold values from -6 to 6
- w_query_rec: bfloat16 [2048, 2048], P('sp', 'tp'), may hold values from -0.125 to 0.125
- w_forget: bfloat16 [2048, 2048], P('sp', 'tp'), may hold values from -0.125 to 0.125
- w_input: bfloat16 [2048, 2048], P('sp', 'tp'), may hold values from -0.125 to 0.125
- forget_gap: float32 [2048], P('tp'), may hold values from 1e-05 to 0.08
- decay_extra: float32 [4096, 16], P('sp', 'tp'), may hold values from -0.75 to 0
- rec_gain: float32 [128], replicated, may hold values from 0.1 to 1.9
- w_q_down: bfloat16 [2048, 512], P(None, 'tp'), may hold values from -0.125 to 0.125
- w_kv_down: bfloat16 [2048, 256], P(None, 'tp'), may hold values from -0.125 to 0.125
- w_key_rope: bfloat16 [2048, 32], replicated, may hold values from -0.125 to 0.125
- q_gain: float32 [512], replicated, may hold values from 1.4 to 7
- kv_gain: float32 [256], replicated, may hold values from 1.4 to 7
- w_q_nope: bfloat16 [512, 1024], P(None, 'tp'), may hold values from -0.25 to 0.25
- w_q_rope: bfloat16 [512, 512], P(None, 'tp'), may hold values from -0.25 to 0.25
- w_k_up: bfloat16 [256, 1024], P(None, 'tp'), may hold values from -0.375 to 0.375
- w_v_up: bfloat16 [256, 1024], P(None, 'tp'), may hold values from -0.375 to 0.375
- w_out_rec: bfloat16 [2048, 2048], P('tp'), may hold values from -0.109375 to 0.109375
- w_out_att: bfloat16 [1024, 2048], P('tp'), may hold values from -0.109375 to 0.109375
Outputs:
- mixed_out: bfloat16 [4096, 2048], P(('sp', 'tp'))
All inputs are finite; a program needn't handle non-finite values.
Results may differ from a plain program's by a relative error of at most 0.02.
The roundings to bfloat16 on the way count: a program that leaves them out, or rounds other values in their place, can miss the bound.
Values may be sent and summed in bfloat16 or wider, within the bound.
A program may use at most 128 MiB of HBM per device.

v0:
```python
import math
import jax
import jax.numpy as jnp
from jax import lax
from jax.sharding import PartitionSpec as P

HG_KDIM = 128
HG_VDIM = 128
HG_BLOCK = 64
NOPE = 64
ROPE = 32
MLA_V = 64
NORM_EPS = 1e-06
ROPE_BASE = 10000.0
NEG_BIG = -1e30


def carried_in(part, axis, combine, identity):
    place = lax.axis_index(axis)
    gathered = jax.tree.map(lambda a: lax.all_gather(a, axis), part)
    state = jax.tree.map(lambda a, e: jnp.zeros_like(a) + jnp.asarray(e, a.dtype), part, identity)

    def one(step, state):
        return combine(
            state, jax.tree.map(lambda a: lax.dynamic_index_in_dim(a, step, 0, False), gathered)
        )

    return lax.fori_loop(0, place, one, state)


def rms_scale(values):
    return values * lax.rsqrt(jnp.mean(values * values, axis=-1, keepdims=True) + NORM_EPS)


def rotate_half(values, cosine, sine_table):
    half_width = values.shape[-1] // 2
    lower_half = values[..., :half_width]
    upper_half = values[..., half_width:]
    return jnp.concatenate(
        [
            lower_half * cosine - upper_half * sine_table,
            lower_half * sine_table + upper_half * cosine,
        ],
        axis=-1,
    )


def rotary_tables(row_count, offset, rot_width):
    positions = jnp.arange(row_count, dtype=jnp.float32) + offset
    frequency = 1.0 / ROPE_BASE ** (jnp.arange(0, rot_width, 2, dtype=jnp.float32) / rot_width)
    angles = positions[:, None] * frequency[None, :]
    return (jnp.cos(angles), jnp.sin(angles))


def block_step(rec_state, inputs):
    queries, key_in, values, log_forget = inputs
    cumulative = jnp.cumsum(log_forget, axis=1)
    log_gaps = cumulative[:, :, None, :] - cumulative[:, None, :, :]
    block_len = queries.shape[1]
    lower_mask = jnp.tril(jnp.ones((block_len, block_len), jnp.float32))
    decays = jnp.exp(jnp.minimum(log_gaps, 0.0)) * lower_mask[None, :, :, None]
    scores = jnp.einsum(
        "htsd,hsd->hts", queries[:, :, None, :] * decays, key_in, precision=lax.Precision.HIGHEST
    )
    block_out = jnp.einsum(
        "hts,hsv->htv", scores, values, precision=lax.Precision.HIGHEST
    ) + jnp.einsum(
        "htd,hdv->htv", queries * jnp.exp(cumulative), rec_state, precision=lax.Precision.HIGHEST
    )
    last_cumul = cumulative[:, -1:, :]
    rec_state = jnp.exp(last_cumul[:, 0, :])[..., None] * rec_state + jnp.einsum(
        "hsd,hsv->hdv",
        key_in * jnp.exp(last_cumul - cumulative),
        values,
        precision=lax.Precision.HIGHEST,
    )
    return (rec_state, block_out)


def score_block(q_nope, q_rope, k_nope, k_rope, values, q_start, k_start):
    score_scale = 1.0 / math.sqrt(NOPE + ROPE)
    scores = (
        jnp.einsum("qhd,khd->hqk", q_nope, k_nope, preferred_element_type=jnp.float32)
        + jnp.einsum("qhr,kr->hqk", q_rope, k_rope, preferred_element_type=jnp.float32)
    ) * score_scale
    q_pos = q_start + jnp.arange(q_nope.shape[0], dtype=jnp.int32)
    k_pos = k_start + jnp.arange(k_nope.shape[0], dtype=jnp.int32)
    allowed = k_pos[None, :] <= q_pos[:, None]
    scores = jnp.where(allowed[None], scores, NEG_BIG)
    block_peak = jnp.max(scores, axis=-1)
    weights = jnp.where(allowed[None], jnp.exp(scores - block_peak[..., None]), 0.0)
    block_total = jnp.sum(weights, axis=-1)
    weights16 = weights.astype(jnp.bfloat16)
    block_sum = jnp.einsum("hqk,khv->hqv", weights16, values, preferred_element_type=jnp.float32)
    return (block_peak, block_total, block_sum)


def merge_terms(earlier, later_part):
    top = jnp.maximum(earlier[0], later_part[0])
    old_factor = jnp.exp(earlier[0] - top)
    new_factor = jnp.exp(later_part[0] - top)
    return (
        top,
        earlier[1] * old_factor + later_part[1] * new_factor,
        earlier[2] * old_factor[..., None] + later_part[2] * new_factor[..., None],
    )


def chain_step(earlier, later_part):
    return (earlier[0] * later_part[0], later_part[0][..., None] * earlier[1] + later_part[1])


def shards(
    hidden_in,
    w_query_rec,
    w_forget,
    w_input,
    forget_gap,
    decay_extra,
    rec_gain,
    w_q_down,
    w_kv_down,
    w_key_rope,
    q_gain,
    kv_gain,
    w_q_nope,
    w_q_rope,
    w_k_up,
    w_v_up,
    w_out_rec,
    w_out_att,
):
    tok_dev = hidden_in.shape[0]
    sp_index = lax.axis_index("sp")
    tp_index = lax.axis_index("tp")
    full_query, full_forget, full_input = (
        lax.all_gather(w_query_rec, "sp", axis=0, tiled=True),
        lax.all_gather(w_forget, "sp", axis=0, tiled=True),
        lax.all_gather(w_input, "sp", axis=0, tiled=True),
    )
    left_weight = jnp.concatenate([full_query, full_forget, full_input], axis=1)
    right_weight = jnp.concatenate([w_q_down, w_kv_down, w_key_rope], axis=1)
    feature_piece = lax.all_gather(hidden_in, "tp", axis=1, tiled=True)
    left_sum = jnp.dot(feature_piece, left_weight, preferred_element_type=jnp.float32)
    right_sum = jnp.dot(feature_piece, right_weight, preferred_element_type=jnp.float32)
    key_cols = full_query.shape[1]
    head_count = key_cols // HG_KDIM
    left_round = left_sum.astype(jnp.bfloat16)
    rec_query = left_round[:, :key_cols].astype(jnp.float32).reshape(tok_dev, head_count, HG_KDIM)
    forget_pre = (
        left_round[:, key_cols : 2 * key_cols]
        .astype(jnp.float32)
        .reshape(tok_dev, head_count, HG_KDIM)
    )
    rec_value = (
        left_round[:, 2 * key_cols :].astype(jnp.float32).reshape(tok_dev, head_count, HG_VDIM)
    )
    gap_rows = forget_gap.reshape(head_count, HG_KDIM)
    closing = jax.nn.sigmoid(-forget_pre)
    key_in = gap_rows * closing
    log_forget = jnp.log1p(-gap_rows * closing) + decay_extra[:, :, None]
    block_count = tok_dev // HG_BLOCK

    def to_blocks(tensor):
        return tensor.reshape(block_count, HG_BLOCK, head_count, tensor.shape[-1]).transpose(
            0, 2, 1, 3
        )

    zero_state = jnp.zeros((head_count, HG_KDIM, HG_VDIM), jnp.float32)
    local_state, local_out = lax.scan(
        block_step,
        zero_state,
        (to_blocks(rec_query), to_blocks(key_in), to_blocks(rec_value), to_blocks(log_forget)),
    )
    local_out = local_out.transpose(0, 2, 1, 3).reshape(tok_dev, head_count, HG_VDIM)
    cumulative = jnp.cumsum(log_forget, axis=0)
    device_decay = jnp.exp(cumulative[-1])
    scanned = carried_in(
        (device_decay, local_state),
        "sp",
        chain_step,
        (jnp.ones_like(device_decay), jnp.zeros_like(local_state)),
    )
    into_state = scanned[1]
    rec_raw = local_out + jnp.einsum(
        "thd,hdv->thv", rec_query * jnp.exp(cumulative), into_state, precision=lax.Precision.HIGHEST
    )
    rec_out = (
        (rms_scale(rec_raw) * rec_gain).astype(jnp.bfloat16).reshape(tok_dev, head_count * HG_VDIM)
    )
    q_cols = w_q_down.shape[1]
    kv_cols = w_kv_down.shape[1]
    right_round = right_sum.astype(jnp.bfloat16)
    q_part = right_round[:, :q_cols]
    kv_part = right_round[:, q_cols : q_cols + kv_cols]
    rope_raw = right_sum[:, q_cols + kv_cols :]
    q_part32 = q_part.astype(jnp.float32)
    kv_part32 = kv_part.astype(jnp.float32)
    square_sums = lax.psum(
        (jnp.sum(q_part32 * q_part32, axis=1), jnp.sum(kv_part32 * kv_part32, axis=1)), "tp"
    )
    q_gain_part = lax.dynamic_slice_in_dim(q_gain, tp_index * q_cols, q_cols, 0)
    kv_gain_part = lax.dynamic_slice_in_dim(kv_gain, tp_index * kv_cols, kv_cols, 0)
    q_norm_part = (
        q_part32 * lax.rsqrt(square_sums[0][:, None] / q_gain.shape[0] + NORM_EPS) * q_gain_part
    ).astype(jnp.bfloat16)
    kv_norm_part = (
        kv_part32 * lax.rsqrt(square_sums[1][:, None] / kv_gain.shape[0] + NORM_EPS) * kv_gain_part
    ).astype(jnp.bfloat16)
    q_normed, latent = (
        lax.all_gather(q_norm_part, "tp", axis=1, tiled=True),
        lax.all_gather(kv_norm_part, "tp", axis=1, tiled=True),
    )
    q_start = sp_index * tok_dev
    cosine, sine_table = rotary_tables(tok_dev, q_start.astype(jnp.float32), ROPE)
    key_rope = rotate_half(rope_raw, cosine, sine_table).astype(jnp.bfloat16)
    att_heads = w_q_nope.shape[1] // NOPE
    q_nope = jnp.dot(q_normed, w_q_nope, preferred_element_type=jnp.float32).astype(jnp.bfloat16)
    q_nope = q_nope.reshape(tok_dev, att_heads, NOPE)
    q_rope = jnp.dot(q_normed, w_q_rope, preferred_element_type=jnp.float32).reshape(
        tok_dev, att_heads, ROPE
    )
    q_rope = rotate_half(q_rope, cosine[:, None, :], sine_table[:, None, :]).astype(jnp.bfloat16)

    def attend(running, latent_rows, rope_rows, key_start):

        def compute(previous):
            k_nope = jnp.dot(latent_rows, w_k_up, preferred_element_type=jnp.float32).astype(
                jnp.bfloat16
            )
            att_value = jnp.dot(latent_rows, w_v_up, preferred_element_type=jnp.float32).astype(
                jnp.bfloat16
            )
            partials = score_block(
                q_nope,
                q_rope,
                k_nope.reshape(-1, att_heads, NOPE),
                rope_rows,
                att_value.reshape(-1, att_heads, MLA_V),
                q_start,
                key_start,
            )
            return merge_terms(previous, partials)

        return lax.cond(key_start <= q_start, compute, lambda previous: previous, running)

    initial_att = (
        jnp.full((att_heads, tok_dev), NEG_BIG, jnp.float32),
        jnp.zeros((att_heads, tok_dev), jnp.float32),
        jnp.zeros((att_heads, tok_dev, MLA_V), jnp.float32),
    )
    latent_piece = lax.all_gather(latent, "sp", axis=0, tiled=True)
    rope_piece = lax.all_gather(key_rope, "sp", axis=0, tiled=True)

    def visit(block_index, current):
        first_row = block_index * tok_dev
        return attend(
            current,
            lax.dynamic_slice_in_dim(latent_piece, first_row, tok_dev, 0),
            lax.dynamic_slice_in_dim(rope_piece, first_row, tok_dev, 0),
            first_row,
        )

    top, total_w, accum = lax.fori_loop(0, latent_piece.shape[0] // tok_dev, visit, initial_att)
    att_out = (accum / total_w[..., None]).transpose(1, 0, 2).reshape(tok_dev, att_heads * MLA_V)
    att_out = att_out.astype(jnp.bfloat16)
    return lax.psum_scatter(
        (
            jnp.dot(rec_out, w_out_rec, preferred_element_type=jnp.float32)
            + jnp.dot(att_out, w_out_att, preferred_element_type=jnp.float32)
        ).astype(jnp.bfloat16),
        "tp",
        scatter_dimension=0,
        tiled=True,
    )


def solution(mesh):
    placed = (
        P("sp", "tp"),
        P("sp", "tp"),
        P("sp", "tp"),
        P("sp", "tp"),
        P("tp"),
        P("sp", "tp"),
        P(),
        P(None, "tp"),
        P(None, "tp"),
        P(),
        P(),
        P(),
        P(None, "tp"),
        P(None, "tp"),
        P(None, "tp"),
        P(None, "tp"),
        P("tp", None),
        P("tp", None),
    )
    return jax.shard_map(
        shards, mesh=mesh, in_specs=placed, out_specs=P(("sp", "tp"), None), check_vma=False
    )
```

profile of v0, /device:TPU:0, one launch (start us, length us, event | category | flops | bytes accessed | tf_op | source)
XLA Modules:
  0.0 698.6 jit_solution(387113204665993834)
XLA Ops:
  11.5 9.2 %all-gather.14.cloned.1.call-done = bf16[256,2048]{1,0:T(8,128)(2,1)} async-done(((bf16[256,1024]{1,0:T(8,128)(2,1)}), bf16[256,2048]{1,0:T(8,128)(2,1)}) %all-gather.14.cloned.1.call-update) | async-done | bytes 1048592 | tf_op jit(solution)/shard_map/all_gather | solution.py:143
  20.7 3.2 fusion.75
  23.9 3.0 all-reduce
  29.2 71.0 %all-gather.8.cloned.1.call-done = bf16[2048,1024]{1,0:T(8,128)(2,1)} async-done(((bf16[128,1024]{1,0:T(8,128)(2,1)}), bf16[2048,1024]{1,0:T(8,128)(2,1)}) %all-gather.8.cloned.1.call-update) | async-done | bytes 4194320 | tf_op jit(solution)/shard_map/all_gather | solution.py:137
  100.2 77.0 %all-gather.10.cloned.1.call-done = bf16[2048,1024]{1,0:T(8,128)(2,1)} async-done(((bf16[128,1024]{1,0:T(8,128)(2,1)}), bf16[2048,1024]{1,0:T(8,128)(2,1)}) %all-gather.10.cloned.1.call-update) | async-done | bytes 4194320 | tf_op jit(solution)/shard_map/all_gather | solution.py:138
  177.2 76.8 %all-gather.12.cloned.1.call-done = bf16[2048,1024]{1,0:T(8,128)(2,1)} async-done(((bf16[128,1024]{1,0:T(8,128)(2,1)}), bf16[2048,1024]{1,0:T(8,128)(2,1)}) %all-gather.12.cloned.1.call-update) | async-done | bytes 4194320 | tf_op jit(solution)/shard_map/all_gather | solution.py:139
  254.1 6.9 fusion.43
  263.8 2.5 copy.75
  266.4 2.4 copy.106
  268.8 2.5 copy.76
  271.3 2.4 copy.107
  273.7 2.5 copy.73
  281.4 164.5 %while.44 = (s32[]{:T(128)}, f32[8,128,128]{2,1,0:T(8,128)S(1)}, f32[4,8,64,128]{3,1,2,0:T(8,128)}, f32[4,8,64,128]{3,1,2,0:T(8,128)}, f32[4,8,64,128]{3,1,2,0:T...) while((s32[]{:T(128)}, f32[8,128,128]{2,1,0:T(8,128)S(1)}, ...), condition=%wide.region_2.3_spmd.clone, body=%wide.region_0.2_spmd.clone.sunk | while | flops 323690496 | bytes 42786940 | solution.py:170
  284.9 3.6 multiply_multiply_fusion.2
  288.6 30.8 %fusion.122 = f32[8,64,1,64]{3,2,1,0:T(1,128)S(1)} fusion(f32[8,64,64,128]{3,2,1,0:T(8,128)S(1)} %multiply_multiply_fusion.2, f32[8,64,128,1]{2,0,1,3:T(8,128)S(1)} %get-tuple-element.728), kind=kOutput, calls=%fused_computation.29.clone.1 | convolution fusion | flops 50331648 | bytes 17170432 | tf_op jit(solution)/shard_map/while/body/eval_jaxpr/htsd,hsd->hts/dot_general | solution.py:62
  326.0 3.6 multiply_multiply_fusion.2
  329.6 30.8 %fusion.122 = f32[8,64,1,64]{3,2,1,0:T(1,128)S(1)} fusion(f32[8,64,64,128]{3,2,1,0:T(8,128)S(1)} %multiply_multiply_fusion.2, f32[8,64,128,1]{2,0,1,3:T(8,128)S(1)} %get-tuple-element.728), kind=kOutput, calls=%fused_computation.29.clone.1 | convolution fusion | flops 50331648 | bytes 17170432 | tf_op jit(solution)/shard_map/while/body/eval_jaxpr/htsd,hsd->hts/dot_general | solution.py:62
  367.1 3.6 multiply_multiply_fusion.2
  370.7 30.8 %fusion.122 = f32[8,64,1,64]{3,2,1,0:T(1,128)S(1)} fusion(f32[8,64,64,128]{3,2,1,0:T(8,128)S(1)} %multiply_multiply_fusion.2, f32[8,64,128,1]{2,0,1,3:T(8,128)S(1)} %get-tuple-element.728), kind=kOutput, calls=%fused_computation.29.clone.1 | convolution fusion | flops 50331648 | bytes 17170432 | tf_op jit(solution)/shard_map/while/body/eval_jaxpr/htsd,hsd->hts/dot_general | solution.py:62
  408.1 3.6 multiply_multiply_fusion.2
  411.8 30.8 %fusion.122 = f32[8,64,1,64]{3,2,1,0:T(1,128)S(1)} fusion(f32[8,64,64,128]{3,2,1,0:T(8,128)S(1)} %multiply_multiply_fusion.2, f32[8,64,128,1]{2,0,1,3:T(8,128)S(1)} %get-tuple-element.728), kind=kOutput, calls=%fused_computation.29.clone.1 | convolution fusion | flops 50331648 | bytes 17170432 | tf_op jit(solution)/shard_map/while/body/eval_jaxpr/htsd,hsd->hts/dot_general | solution.py:62
  453.1 44.3 %all_gather.44 = bf16[4096,32]{0,1:T(8,128)(2,1)} all-gather(bf16[256,32]{0,1:T(8,128)(2,1)S(1)} %pad_maximum_fusion.1), channel_id=1, replica_groups=mesh['sp'=16,'tp'=2] {'sp'}, dimensions={0}, use_global_device_ids=true | all-gather | bytes 278528 | tf_op jit(solution)/shard_map/all_gather | solution.py:253
  497.4 4.1 copy.90
  501.5 7.4 %while.43 = (s32[]{:T(128)}, f32[8,256]{1,0:T(8,128)S(1)}, f32[8,256]{1,0:T(8,128)S(1)}, f32[8,256,64]{1,2,0:T(8,128)S(1)}, s32[]{:T(128)}, /*index=5*/bf16[4096...) while((s32[]{:T(128)}, f32[8,256]{1,0:T(8,128)S(1)}, ...), condition=%wide.region_17.18_spmd, body=%wide.region_12.17_spmd.sunk | while | flops 307962368 | bytes 15733113 | solution.py:264
  501.5 6.7 conditional.2
  509.0 2.4 fusion.64
  516.2 2.1 slice.61
  519.6 2.7 copy.87
  522.2 136.0 %all_gather.38 = f32[16,8,128]{2,1,0:T(8,128)S(1)} all-gather(f32[1,8,128]{2,1,0:T(8,128)S(1)} %exp.49), channel_id=1, replica_groups=mesh['sp'=16,'tp'=2] {'sp'}, dimensions={0}, use_global_device_ids=true | all-gather | bytes 69632 | tf_op jit(solution)/shard_map/all_gather | solution.py:20
  658.2 2.9 copy_multiply_fusion
  661.2 3.0 multiply_reduce_fusion
  667.4 24.3 %reduce-scatter.2.cloned.1.call-done = bf16[128,2048]{1,0:T(8,128)(2,1)} async-done(((bf16[256,2048]{1,0:T(8,128)(2,1)}), bf16[128,2048]{1,0:T(8,128)(2,1)}) %reduce-scatter.2.cloned.1.call-update) | async-done | bytes 524304 | tf_op jit(solution)/shard_map/reduce_scatter | solution.py:267
  (168 shorter events, 64.6 us)
Async XLA Ops:
  6.5 659.1 %copy-start = (bf16[512,2048]{1,0:T(8,128)(2,1)S(1)}, bf16[512,2048]{1,0:T(8,128)(2,1)}, u32[]{:S(2)}) copy-start(bf16[512,2048]{1,0:T(8,128)(2,1)} %param.43) | copy-start | bytes 6291460
  6.5 4.9 copy-start.14
  6.5 5.0 copy-start.9
  6.5 14.1 %all-gather.14.cloned.1.call-start = ((), (), s32[]{:S(2)}) async-start(), calls=%async_computation.4 | async-start | bytes 1572864 | tf_op jit(solution)/shard_map/all_gather | solution.py:143
  7.3 93.0 %all-gather.8.cloned.1.call-start = ((), (), s32[]{:S(2)}) async-start(), calls=%async_computation.1 | async-start | bytes 4456448 | tf_op jit(solution)/shard_map/all_gather | solution.py:137
  8.0 169.2 %all-gather.10.cloned.1.call-start = ((), (), s32[]{:S(2)}) async-start(), calls=%async_computation.2 | async-start | bytes 4456448 | tf_op jit(solution)/shard_map/all_gather | solution.py:138
  8.7 245.3 %all-gather.12.cloned.1.call-start = ((), (), s32[]{:S(2)}) async-start(), calls=%async_computation.3 | async-start | bytes 4456448 | tf_op jit(solution)/shard_map/all_gather | solution.py:139
  9.3 488.1 %all-gather.16.cloned.1.call-start = ((), (), s32[]{:S(2)}) async-start(), calls=%async_computation.5 | async-start | bytes 2228224 | tf_op jit(solution)/shard_map/all_gather | solution.py:252
  11.5 268.1 %copy-start.7 = (f32[8,128]{1,0:T(8,128)}, f32[8,128]{1,0:T(8,128)S(1)}, u32[]{:S(2)}) copy-start(f32[8,128]{1,0:T(8,128)S(1)} %bitcast_negate_fusion) | copy-start | bytes 12292
  29.1 631.9 %all-gather.18.cloned.1.call-start = ((), (), s32[]{:S(2)}) async-start(), calls=%async_computation.7 | async-start | bytes 8912896 | tf_op jit(solution)/shard_map/all_gather | solution.py:20
  276.3 1.6 copy-start.4
  276.3 1.9 copy-start.5
  281.3 165.4 %copy-start.8 = (f32[8,128]{1,0:T(8,128)S(1)}, f32[8,128]{1,0:T(8,128)}, u32[]{:S(2)}) copy-start(f32[8,128]{1,0:T(8,128)} %copy-done.7) | copy-start | bytes 12292
  281.3 165.5 %copy-start.12 = (f32[512]{0:T(512)S(1)}, f32[512]{0:T(512)}, u32[]{:S(2)}) copy-start(f32[512]{0:T(512)} %param.36) | copy-start | bytes 6148
  281.3 165.6 %copy-start.10 = (f32[256]{0:T(256)S(1)}, f32[256]{0:T(256)}, u32[]{:S(2)}) copy-start(f32[256]{0:T(256)} %get-tuple-element.540) | copy-start | bytes 3076
  281.3 167.7 %copy-start.6 = (bf16[512,512]{1,0:T(8,128)(2,1)S(1)}, bf16[512,512]{1,0:T(8,128)(2,1)}, u32[]{:S(2)}) copy-start(bf16[512,512]{1,0:T(8,128)(2,1)} %param.38) | copy-start | bytes 1572868
  445.8 0.8 copy-start.1
  446.7 245.1 %reduce-scatter.2.cloned.1.call-start = ((), (), s32[]{:S(2)}) async-start(), calls=%async_computation.6 | async-start | bytes 1572864 | tf_op jit(solution)/shard_map/reduce_scatter | solution.py:267
  504.5 1.5 copy-start.3
  516.2 142.0 %copy-start.2 = (f32[256,1024]{0,1:T(8,128)S(1)}, f32[256,1024]{0,1:T(8,128)}, u32[]{:S(2)}) copy-start(f32[256,1024]{0,1:T(8,128)} %get-tuple-element.554) | copy-start | bytes 3145732
  661.1 3.1 copy-start.11
  661.1 3.2 copy-start.13
Sparse Core Ops, SparseCore 0:
  8.9 11.7 all-gather.13
  23.4 76.7 all-gather.7
  103.0 74.1 all-gather.9
  179.9 74.1 all-gather.11
  256.6 63.3 all-gather.15
  446.8 112.9 all-gather.17
  667.6 24.1 reduce-scatter.1
where the time goes:
time: 702 us; the launch traced here: 699 us
  waiting for transfers between devices  261 us (37%)
  blocking collectives  187 us (27%)
  matrix products  156 us (22%)
  local copies, waits for them, and re-layouts  41.7 us (6%)
  other arithmetic  37 us (5%)
  between operations  13.8 us (2%)
    all_gather x1, blocking collectives, carried_in(): gathered = jax.tree.map(lambda a: lax.all_gather(a, axis), part)  136 us
    dot_general x4, matrix products, block_step(): jnp.einsum('htsd,hsd->hts', queries[:, :, None, :] * decays, key_in, prec...  123 us
    all_gather x1, waiting for transfers between devices, shards(): lax.all_gather(w_forget, 'sp', axis=0, tiled=True)  77 us
    all_gather x1, waiting for transfers between devices, shards(): lax.all_gather(w_input, 'sp', axis=0, tiled=True)  76.8 us
    all_gather x1, waiting for transfers between devices, shards(): lax.all_gather(w_query_rec, 'sp', axis=0, tiled=True)  71 us
    all_gather x1, blocking collectives, shards(): rope_piece = lax.all_gather(key_rope, 'sp', axis=0, tiled=True)  44.3 us
    reduce_scatter x1, waiting for transfers between devices, shards(): lax.psum_scatter((jnp.dot(rec_out, w_out_rec, preferred_element_type=jnp....  24.3 us
    mul x4, other arithmetic, block_step(): queries[:, :, None, :] * decays  14.5 us
  transfers between devices with their start and end apart: 7, of which 5 were waited for; matrix products, arithmetic and copies ran while one was open for 33% of the time, Pallas kernels for 0%

commit v1 on v0

--- a/solution.py
+++ b/solution.py
@@ -249,8 +249,11 @@
         jnp.zeros((att_heads, tok_dev), jnp.float32),
         jnp.zeros((att_heads, tok_dev, MLA_V), jnp.float32),
     )
-    latent_piece = lax.all_gather(latent, "sp", axis=0, tiled=True)
-    rope_piece = lax.all_gather(key_rope, "sp", axis=0, tiled=True)
+    latent_piece, rope_piece = jnp.split(
+        lax.all_gather(jnp.concatenate([latent, key_rope], axis=1), "sp", axis=0, tiled=True),
+        [latent.shape[1]],
+        axis=1,
+    )
 
     def visit(block_index, current):
         first_row = block_index * tok_dev

time: 702 us -> 665 us (0.947)
  blocking collectives: 187 us -> 146 us
    all_gather x1 -> x0, blocking collectives: 44.3 us -> none  [shards(): rope_piece = lax.all_gather(key_rope, 'sp', axis=0, tiled=True)]
  transfers between devices with their start and end apart: 7 -> 7, of which waited for: 5 -> 5; matrix products, arithmetic and copies ran while one was open for 33% -> 35% of each run, Pallas kernels for 0% -> 0%
where the time goes in v1:
time: 665 us; the launch traced here: 661 us
  waiting for transfers between devices  258 us (39%)
  matrix products  156 us (23%)
  blocking collectives  146 us (22%)
  local copies, waits for them, and re-layouts  47.1 us (7%)
  other arithmetic  38.7 us (6%)
  between operations  13.8 us (2%)
    all_gather x1, blocking collectives, carried_in(): gathered = jax.tree.map(lambda a: lax.all_gather(a, axis), part)  139 us
    dot_general x4, matrix products, block_step(): jnp.einsum('htsd,hsd->hts', queries[:, :, None, :] * decays, key_in, prec...  123 us
    all_gather x1, waiting for transfers between devices, shards(): lax.all_gather(w_forget, 'sp', axis=0, tiled=True)  77 us
    all_gather x1, waiting for transfers between devices, shards(): lax.all_gather(w_input, 'sp', axis=0, tiled=True)  76.8 us
    all_gather x1, waiting for transfers between devices, shards(): lax.all_gather(w_query_rec, 'sp', axis=0, tiled=True)  69.1 us
    reduce_scatter x1, waiting for transfers between devices, shards(): lax.psum_scatter((jnp.dot(rec_out, w_out_rec, preferred_element_type=jnp....  24.3 us
    mul x4, other arithmetic, block_step(): queries[:, :, None, :] * decays  14.5 us
  transfers between devices with their start and end apart: 7, of which 5 were waited for; matrix products, arithmetic and copies ran while one was open for 35% of the time, Pallas kernels for 0%

profile of v1, /device:TPU:0, one launch (start us, length us, event | category | flops | bytes accessed | tf_op | source)
XLA Modules:
  0.0 661.3 jit_solution(6687738025380617596)
XLA Ops:
  12.9 7.8 %all-gather.14.cloned.1.call-done = bf16[256,2048]{1,0:T(8,128)(2,1)} async-done(((bf16[256,1024]{1,0:T(8,128)(2,1)}), bf16[256,2048]{1,0:T(8,128)(2,1)}) %all-gather.14.cloned.1.call-update) | async-done | bytes 1048592 | tf_op jit(solution)/shard_map/all_gather | solution.py:143
  20.7 3.2 fusion.75
  23.9 3.0 all-reduce
  31.2 69.1 %all-gather.8.cloned.1.call-done = bf16[2048,1024]{1,0:T(8,128)(2,1)} async-done(((bf16[128,1024]{1,0:T(8,128)(2,1)}), bf16[2048,1024]{1,0:T(8,128)(2,1)}) %all-gather.8.cloned.1.call-update) | async-done | bytes 4194320 | tf_op jit(solution)/shard_map/all_gather | solution.py:137
  100.2 77.0 %all-gather.10.cloned.1.call-done = bf16[2048,1024]{1,0:T(8,128)(2,1)} async-done(((bf16[128,1024]{1,0:T(8,128)(2,1)}), bf16[2048,1024]{1,0:T(8,128)(2,1)}) %all-gather.10.cloned.1.call-update) | async-done | bytes 4194320 | tf_op jit(solution)/shard_map/all_gather | solution.py:138
  177.2 76.8 %all-gather.12.cloned.1.call-done = bf16[2048,1024]{1,0:T(8,128)(2,1)} async-done(((bf16[128,1024]{1,0:T(8,128)(2,1)}), bf16[2048,1024]{1,0:T(8,128)(2,1)}) %all-gather.12.cloned.1.call-update) | async-done | bytes 4194320 | tf_op jit(solution)/shard_map/all_gather | solution.py:139
  254.1 6.9 %fusion.43 = bf16[256,3072]{0,1:T(8,128)(2,1)S(1)} fusion(bf16[256,2048]{1,0:T(8,128)(2,1)} %all-gather.14.cloned.1.call-done, bf16[2048,1024]{1,0:T(8,128)(2,1)} %all-gather.12.cloned.1.call-done, bf16[2048,1024]{1,0:T(8,128)(2,1)} %all-gather.10.cloned.1.call-done, bf16[2048,1024]{1,0:T(8,128)(2,1)} %all-gather.8.cloned.1.call-done), kind=kOutput, calls=%fused_computation.65 | convolution fusion | flops 3259760640 | bytes 15204352 | tf_op jit(solution)/shard_map/dot_general | solution.py:144
  263.8 2.6 copy.75
  266.3 2.4 copy.106
  268.8 2.5 copy.76
  271.3 2.4 copy.107
  273.7 2.5 copy.73
  281.3 164.5 %while.44 = (s32[]{:T(128)}, f32[8,128,128]{2,1,0:T(8,128)S(1)}, f32[4,8,64,128]{3,1,2,0:T(8,128)}, f32[4,8,64,128]{3,1,2,0:T(8,128)}, f32[4,8,64,128]{3,1,2,0:T...) while((s32[]{:T(128)}, f32[8,128,128]{2,1,0:T(8,128)S(1)}, ...), condition=%wide.region_2.3_spmd.clone, body=%wide.region_0.2_spmd.clone.sunk | while | flops 323690496 | bytes 42786940 | solution.py:170
  284.9 3.6 multiply_multiply_fusion.2
  288.5 30.8 %fusion.122 = f32[8,64,1,64]{3,2,1,0:T(1,128)S(1)} fusion(f32[8,64,64,128]{3,2,1,0:T(8,128)S(1)} %multiply_multiply_fusion.2, f32[8,64,128,1]{2,0,1,3:T(8,128)S(1)} %get-tuple-element.728), kind=kOutput, calls=%fused_computation.29.clone.1 | convolution fusion | flops 50331648 | bytes 17170432 | tf_op jit(solution)/shard_map/while/body/eval_jaxpr/htsd,hsd->hts/dot_general | solution.py:62
  325.9 3.6 multiply_multiply_fusion.2
  329.6 30.8 %fusion.122 = f32[8,64,1,64]{3,2,1,0:T(1,128)S(1)} fusion(f32[8,64,64,128]{3,2,1,0:T(8,128)S(1)} %multiply_multiply_fusion.2, f32[8,64,128,1]{2,0,1,3:T(8,128)S(1)} %get-tuple-element.728), kind=kOutput, calls=%fused_computation.29.clone.1 | convolution fusion | flops 50331648 | bytes 17170432 | tf_op jit(solution)/shard_map/while/body/eval_jaxpr/htsd,hsd->hts/dot_general | solution.py:62
  367.0 3.6 multiply_multiply_fusion.2
  370.6 30.8 %fusion.122 = f32[8,64,1,64]{3,2,1,0:T(1,128)S(1)} fusion(f32[8,64,64,128]{3,2,1,0:T(8,128)S(1)} %multiply_multiply_fusion.2, f32[8,64,128,1]{2,0,1,3:T(8,128)S(1)} %get-tuple-element.728), kind=kOutput, calls=%fused_computation.29.clone.1 | convolution fusion | flops 50331648 | bytes 17170432 | tf_op jit(solution)/shard_map/while/body/eval_jaxpr/htsd,hsd->hts/dot_general | solution.py:62
  408.1 3.6 multiply_multiply_fusion.2
  411.7 30.8 %fusion.122 = f32[8,64,1,64]{3,2,1,0:T(1,128)S(1)} fusion(f32[8,64,64,128]{3,2,1,0:T(8,128)S(1)} %multiply_multiply_fusion.2, f32[8,64,128,1]{2,0,1,3:T(8,128)S(1)} %get-tuple-element.728), kind=kOutput, calls=%fused_computation.29.clone.1 | convolution fusion | flops 50331648 | bytes 17170432 | tf_op jit(solution)/shard_map/while/body/eval_jaxpr/htsd,hsd->hts/dot_general | solution.py:62
  452.1 3.3 split.8
  455.4 4.1 copy.90
  461.2 7.4 %while.43 = (s32[]{:T(128)}, f32[8,256]{1,0:T(8,128)S(1)}, f32[8,256]{1,0:T(8,128)S(1)}, f32[8,256,64]{1,2,0:T(8,128)S(1)}, s32[]{:T(128)}, /*index=5*/bf16[4096...) while((s32[]{:T(128)}, f32[8,256]{1,0:T(8,128)S(1)}, ...), condition=%wide.region_17.18_spmd, body=%wide.region_12.17_spmd.sunk | while | flops 307962368 | bytes 15733113 | solution.py:267
  461.2 6.7 %conditional.2 = ((f32[8,256]{1,0:T(8,128)S(1)}, f32[8,256]{1,0:T(8,128)S(1)}, f32[8,256,64]{1,2,0:T(8,128)S(1)})) conditional(s32[]{:T(128)} %convert_element_type.125, (f32[8,256]{1,0:T(8,128)S(1)}, f32[8,256]{1,0:T(8,128)S(1)}, f32[8,256,64]{1,2,0:T(8,128)S(1)}) %tuple.104, (s32[]{:T(128)}, s32[]{:T(128)}, bf16[4096,256]{1,0:T(8,128)(2,1)}, ...), branch_computations={%region_13.13_spmd, %region_14.16_spmd} | conditional | flops 307962368 | bytes 15732850 | solution.py:245
  468.6 2.1 fusion.64
  475.4 2.1 slice.61
  478.8 2.6 copy.87
  481.4 139.4 %all_gather.35 = f32[16,8,128]{2,1,0:T(8,128)S(1)} all-gather(f32[1,8,128]{2,1,0:T(8,128)S(1)} %exp.49), channel_id=1, replica_groups=mesh['sp'=16,'tp'=2] {'sp'}, dimensions={0}, use_global_device_ids=true | all-gather | bytes 69632 | tf_op jit(solution)/shard_map/all_gather | solution.py:20
  620.8 3.0 copy_multiply_fusion
  623.8 3.0 multiply_reduce_fusion
  630.1 24.3 %reduce-scatter.2.cloned.1.call-done = bf16[128,2048]{1,0:T(8,128)(2,1)} async-done(((bf16[256,2048]{1,0:T(8,128)(2,1)}), bf16[128,2048]{1,0:T(8,128)(2,1)}) %reduce-scatter.2.cloned.1.call-update) | async-done | bytes 524304 | tf_op jit(solution)/shard_map/reduce_scatter | solution.py:270
  (171 shorter events, 68.5 us)
Async XLA Ops:
  6.5 621.8 %copy-start = (bf16[512,2048]{1,0:T(8,128)(2,1)S(1)}, bf16[512,2048]{1,0:T(8,128)(2,1)}, u32[]{:S(2)}) copy-start(bf16[512,2048]{1,0:T(8,128)(2,1)} %param.43) | copy-start | bytes 6291460
  6.5 14.1 %all-gather.14.cloned.1.call-start = ((), (), s32[]{:S(2)}) async-start(), calls=%async_computation.4 | async-start | bytes 1572864 | tf_op jit(solution)/shard_map/all_gather | solution.py:143
  7.3 93.0 %all-gather.8.cloned.1.call-start = ((), (), s32[]{:S(2)}) async-start(), calls=%async_computation.1 | async-start | bytes 4456448 | tf_op jit(solution)/shard_map/all_gather | solution.py:137
  8.0 169.2 %all-gather.10.cloned.1.call-start = ((), (), s32[]{:S(2)}) async-start(), calls=%async_computation.2 | async-start | bytes 4456448 | tf_op jit(solution)/shard_map/all_gather | solution.py:138
  8.7 245.3 %all-gather.12.cloned.1.call-start = ((), (), s32[]{:S(2)}) async-start(), calls=%async_computation.3 | async-start | bytes 4456448 | tf_op jit(solution)/shard_map/all_gather | solution.py:139
  9.3 442.8 %all-gather.16.cloned.1.call-start = ((), (), s32[]{:S(2)}) async-start(), calls=%async_computation.5 | async-start | bytes 2506752 | tf_op jit(solution)/shard_map/all_gather | solution.py:253
  12.9 266.7 %copy-start.9 = (f32[8,128]{1,0:T(8,128)}, f32[8,128]{1,0:T(8,128)S(1)}, u32[]{:S(2)}) copy-start(f32[8,128]{1,0:T(8,128)S(1)} %bitcast_negate_fusion) | copy-start | bytes 12292
  31.1 592.6 %all-gather.18.cloned.1.call-start = ((), (), s32[]{:S(2)}) async-start(), calls=%async_computation.7 | async-start | bytes 8912896 | tf_op jit(solution)/shard_map/all_gather | solution.py:20
  276.2 1.6 copy-start.4
  276.2 1.9 copy-start.5
  277.8 1.7 copy-start.11
  281.3 165.4 %copy-start.10 = (f32[8,128]{1,0:T(8,128)S(1)}, f32[8,128]{1,0:T(8,128)}, u32[]{:S(2)}) copy-start(f32[8,128]{1,0:T(8,128)} %copy-done.9) | copy-start | bytes 12292
  281.3 165.5 %copy-start.14 = (f32[512]{0:T(512)S(1)}, f32[512]{0:T(512)}, u32[]{:S(2)}) copy-start(f32[512]{0:T(512)} %param.36) | copy-start | bytes 6148
  281.3 165.6 %copy-start.12 = (f32[256]{0:T(256)S(1)}, f32[256]{0:T(256)}, u32[]{:S(2)}) copy-start(f32[256]{0:T(256)} %get-tuple-element.540) | copy-start | bytes 3076
  281.3 167.7 %copy-start.6 = (bf16[512,512]{1,0:T(8,128)(2,1)S(1)}, bf16[512,512]{1,0:T(8,128)(2,1)}, u32[]{:S(2)}) copy-start(bf16[512,512]{1,0:T(8,128)(2,1)} %param.38) | copy-start | bytes 1572868
  445.8 0.8 copy-start.1
  445.8 5.6 copy-start.7
  445.8 5.6 copy-start.8
  446.6 207.8 %reduce-scatter.2.cloned.1.call-start = ((), (), s32[]{:S(2)}) async-start(), calls=%async_computation.6 | async-start | bytes 1572864 | tf_op jit(solution)/shard_map/reduce_scatter | solution.py:270
  464.2 1.5 copy-start.3
  475.4 145.3 %copy-start.2 = (f32[256,1024]{0,1:T(8,128)S(1)}, f32[256,1024]{0,1:T(8,128)}, u32[]{:S(2)}) copy-start(f32[256,1024]{0,1:T(8,128)} %get-tuple-element.554) | copy-start | bytes 3145732
  623.8 3.1 copy-start.13
  623.8 3.2 copy-start.15
Sparse Core Ops, SparseCore 0:
  8.9 11.7 all-gather.13
  23.4 76.7 all-gather.7
  103.0 74.1 all-gather.9
  179.9 74.1 all-gather.11
  256.6 66.2 all-gather.15
  446.7 111.0 all-gather.17
  630.2 24.1 reduce-scatter.1
